TPU v7x, 512 devices: a whole 4x8x8 slice. The times are simulated.
512 devices in a mesh: ep: 128 (over z, y, core), tp: 4 (over x).
Axes of the slice: x: 4, y: 8, z: 8, core: 2. Of those that a mesh axis runs over, the one named last changes fastest.
Arguments:
- tokens: bfloat16 [16384, 2048], P('ep'), may hold values from -24 to 24
- cotangent: bfloat16 [16384, 2048], P('ep'), may hold values from -6 to 6
- routing: int32 [16384, 2], P('ep'), may hold values from 0 to 127, all different within a row; in each aligned block of 128 rows (0 to 127, 128 to 255, ...) at most 4 rows name the same one
- router_weight: bfloat16 [2048, 128], replicated, may hold values from -0.125 to 0.125
- gate_weight: bfloat16 [128, 2048, 512], P('ep', None, 'tp'), may hold values from -0.125 to 0.125
- up_weight: bfloat16 [128, 2048, 512], P('ep', None, 'tp'), may hold values from -0.125 to 0.125
- down_weight: bfloat16 [128, 512, 2048], P('ep', 'tp'), may hold values from -0.25 to 0.25
Outputs:
- grad_tokens: bfloat16 [16384, 2048], P('ep', 'tp')
- grad_gating: float32 [16384, 2], P('ep')
- grad_router: float32 [2048, 128], P('ep')
- grad_gate_weight: bfloat16 [128, 2048, 512], P('ep', None, 'tp')
- grad_up_weight: bfloat16 [128, 2048, 512], P('ep', None, 'tp')
- grad_down_weight: bfloat16 [128, 512, 2048], P('ep', 'tp')
- in_norms: float32 [128, 2, 2048], P('ep')
- down_norms: float32 [128, 512], P('ep', 'tp')
- router_norms: float32 [2048], P('ep')
Inputs may be any that keep to these rules, and one draw needn't show every extreme that they name: `routing`: each row names 2 different experts. Among the rows of one index of ep no expert is named by more than 4 rows, a bound that some block reaches in some of them.
All inputs are finite; a program needn't handle non-finite values.
Results may differ from a plain program's by a relative error of at most 0.014.
Values may be sent and summed in bfloat16 or wider, within the bound.
A program may use at most 64 MiB of HBM per device.

v0:
```python
import jax
import jax.numpy as jnp
from jax import lax
from jax.sharding import Mesh
from jax.sharding import PartitionSpec as P

EP = ("ep_0", "ep_1", "ep_2")


def side_by_side(arrays, axis, split_dim, concat_dim, along):
    ends, at = ([], 0)
    for a in arrays[:-1]:
        at += a.shape[along]
        ends.append(at)
    both = jnp.concatenate(arrays, axis=along)
    return tuple(
        jnp.split(
            lax.all_to_all(both, axis, split_axis=split_dim, concat_axis=concat_dim, tiled=True),
            ends,
            axis=along,
        )
    )


def side_by_side_2(arrays, axis, dim, along):
    ends, at = ([], 0)
    for a in arrays[:-1]:
        at += a.shape[along]
        ends.append(at)
    both = jnp.concatenate(arrays, axis=along)
    return tuple(jnp.split(lax.all_gather(both, axis, axis=dim, tiled=True), ends, axis=along))


def split_up(array, dim, count):
    before, after = (array.shape[:dim], array.shape[dim + 1 :])
    return jnp.moveaxis(array.reshape(*before, count, -1, *after), dim, 0)


def sum_at_owner(array, axis, dim):
    blocks = split_up(array, dim, lax.axis_size(axis))
    arrived = lax.all_to_all(blocks, axis, split_axis=0, concat_axis=0, tiled=True)
    return arrived.astype(jnp.float32).sum(axis=0)


def copy_for_each(array, axis):
    count = lax.axis_size(axis)
    return lax.all_to_all(
        jnp.broadcast_to(array[None], (count, *array.shape)), axis, 0, 0, tiled=True
    )


def over_copies(array, axis):
    return copy_for_each(array, axis).sum(axis=0)


def packed_total(arrays, axis):
    ends = [0]
    for a in arrays:
        ends.append(ends[-1] + a.size)
    total = over_copies(jnp.concatenate([a.ravel() for a in arrays]), axis)
    return tuple((total[b:e].reshape(a.shape) for a, b, e in zip(arrays, ends, ends[1:])))


def sum_in_order(blocks, axes, sequence):
    inside = blocks.shape[1:]
    blocks = blocks.reshape(*(lax.axis_size(a) for a in axes), *inside)
    blocks = jnp.moveaxis(blocks, sequence, range(len(axes))).reshape(-1, *inside)
    for k in sequence:
        blocks = lax.psum_scatter(blocks, axes[k], scatter_dimension=0, tiled=True)
    return blocks[0]


def scatter_axes(array, axes, sequence, dim):
    count = lax.axis_size(axes)
    return sum_in_order(split_up(array, dim, count), axes, sequence)


def silu_parts(pre_gate):
    sigmoid_gate = jax.nn.sigmoid(pre_gate)
    return (pre_gate * sigmoid_gate, sigmoid_gate * (1.0 + pre_gate * (1.0 - sigmoid_gate)))


def slot_layout(routing, experts_all, capacity):
    tok_count, top_count = routing.shape
    flat_expert = routing.reshape(-1)
    one_hot = (flat_expert[:, None] == jnp.arange(experts_all, dtype=jnp.int32)[None, :]).astype(
        jnp.int32
    )
    earlier = jnp.cumsum(one_hot, axis=0) - one_hot
    within = jnp.sum(earlier * one_hot, axis=1)
    position = flat_expert * capacity + within
    vacant = jnp.full((experts_all * capacity,), tok_count * top_count, jnp.int32)
    return (vacant.at[position].set(jnp.arange(tok_count * top_count, dtype=jnp.int32)), position)


def shards(tokens, cotangent, routing, router_weight, gate_weight, up_weight, down_weight):
    tok_count, model_width = tokens.shape
    top_count = routing.shape[1]
    experts_all = router_weight.shape[1]
    expert_local = gate_weight.shape[0]
    ep_size = lax.axis_size(EP)
    tp_size = lax.axis_size("tp")
    tp_index = lax.axis_index("tp")
    slice_width = model_width // tp_size
    capacity = max(2, 2 * tok_count * top_count // experts_all)
    arrived = ep_size * capacity
    logits = jnp.dot(tokens, router_weight, preferred_element_type=jnp.float32)
    picked = (
        routing[:, :, None] == jnp.arange(experts_all, dtype=jnp.int32)[None, None, :]
    ).astype(jnp.float32)
    scores = jax.nn.sigmoid(jnp.einsum("tke,te->tk", picked, logits))
    score_sum = jnp.sum(scores, axis=1, keepdims=True)
    gating = scores / score_sum
    assignment, position = slot_layout(routing, experts_all, capacity)
    source_row = assignment // top_count
    padded_tokens = jnp.concatenate([tokens, jnp.zeros((1, model_width), tokens.dtype)], axis=0)
    padded_cotangent = jnp.concatenate(
        [cotangent, jnp.zeros((1, model_width), cotangent.dtype)], axis=0
    )
    padded_gating = jnp.concatenate([gating.reshape(-1), jnp.zeros((1,), jnp.float32)])
    sent_gating = padded_gating[assignment].reshape(experts_all, capacity)
    own_tokens = lax.dynamic_slice_in_dim(padded_tokens, tp_index * slice_width, slice_width, 1)
    own_cotangent = lax.dynamic_slice_in_dim(
        padded_cotangent, tp_index * slice_width, slice_width, 1
    )
    part_tokens, part_cotangent = side_by_side(
        (
            own_tokens[source_row].reshape(experts_all, capacity, slice_width),
            own_cotangent[source_row].reshape(experts_all, capacity, slice_width),
        ),
        EP,
        0,
        0,
        1,
    )
    got_tokens, got_cotangent = side_by_side_2((part_tokens, part_cotangent), "tp", 2, 0)
    got_gating = lax.all_to_all(sent_gating, EP, split_axis=0, concat_axis=0, tiled=True)

    def by_expert(values):
        shaped = values.reshape((ep_size, expert_local) + values.shape[1:])
        return jnp.moveaxis(shaped, 1, 0).reshape((expert_local, arrived) + values.shape[2:])

    def by_source(values):
        shaped = values.reshape((expert_local, ep_size, capacity) + values.shape[2:])
        return jnp.moveaxis(shaped, 1, 0).reshape(
            (ep_size * expert_local, capacity) + values.shape[2:]
        )

    rows_in = by_expert(got_tokens)
    cot_rows = by_expert(got_cotangent)
    slot_gating = by_expert(got_gating)[:, :, None]
    pre_gate = jnp.einsum("lrd,ldf->lrf", rows_in, gate_weight, preferred_element_type=jnp.float32)
    pre_up = jnp.einsum("lrd,ldf->lrf", rows_in, up_weight, preferred_element_type=jnp.float32)
    activated, silu_slope = silu_parts(pre_gate)
    hidden = (activated * pre_up).astype(jnp.bfloat16)
    back_raw = jnp.einsum("lrd,lfd->lrf", cot_rows, down_weight, preferred_element_type=jnp.float32)
    hidden_wide = hidden.astype(jnp.float32)
    gate_partial = jnp.sum(hidden_wide * back_raw, axis=2)
    scaled_back = slot_gating * back_raw
    grad_pre_gate = (scaled_back * pre_up * silu_slope).astype(jnp.bfloat16)
    grad_pre_up = (scaled_back * activated).astype(jnp.bfloat16)
    scaled_hidden = (slot_gating * hidden_wide).astype(jnp.bfloat16)
    gate_sum = jnp.einsum(
        "lrd,lrf->ldf", rows_in, grad_pre_gate, preferred_element_type=jnp.float32
    )
    up_sum = jnp.einsum("lrd,lrf->ldf", rows_in, grad_pre_up, preferred_element_type=jnp.float32)
    down_sum = jnp.einsum(
        "lrf,lrd->lfd", scaled_hidden, cot_rows, preferred_element_type=jnp.float32
    )
    down_norms = jnp.sum(down_sum * down_sum, axis=2)
    back_partial = jnp.einsum(
        "lrf,ldf->lrd", grad_pre_gate, gate_weight, preferred_element_type=jnp.float32
    ) + jnp.einsum("lrf,ldf->lrd", grad_pre_up, up_weight, preferred_element_type=jnp.float32)
    back_rounded = back_partial.astype(jnp.bfloat16)
    slot_values = sum_at_owner(back_rounded, "tp", 2).astype(jnp.bfloat16)
    gating_total, gate_rows, up_rows = packed_total(
        (gate_partial, jnp.sum(gate_sum * gate_sum, axis=2), jnp.sum(up_sum * up_sum, axis=2)), "tp"
    )
    home_values = lax.all_to_all(
        by_source(slot_values), EP, split_axis=0, concat_axis=0, tiled=True
    )
    home_gating = lax.all_to_all(
        by_source(gating_total), EP, split_axis=0, concat_axis=0, tiled=True
    )
    flat_values = home_values.reshape(experts_all * capacity, slice_width)
    token_terms = (
        flat_values[position].reshape(tok_count, top_count, slice_width).astype(jnp.float32)
    )
    grad_gating = home_gating.reshape(-1)[position].reshape(tok_count, top_count)
    weighted = jnp.sum(gating * grad_gating, axis=1, keepdims=True)
    grad_scores = (grad_gating - weighted) / score_sum
    grad_chosen = grad_scores * scores * (1.0 - scores)
    grad_logits = jnp.einsum("tk,tke->te", grad_chosen, picked).astype(jnp.bfloat16)
    router_slice = lax.dynamic_slice_in_dim(router_weight, tp_index * slice_width, slice_width, 0)
    router_term = jnp.einsum(
        "te,de->td", grad_logits, router_slice, preferred_element_type=jnp.float32
    )
    grad_tokens = (jnp.sum(token_terms, axis=1) + router_term).astype(jnp.bfloat16)
    grad_router = scatter_axes(
        jnp.einsum("td,te->de", tokens, grad_logits, preferred_element_type=jnp.float32),
        EP,
        (2, 0, 1),
        0,
    )
    router_norms = jnp.sum(grad_router * grad_router, axis=1)
    in_norms = jnp.stack([gate_rows, up_rows], axis=1)
    return (
        grad_tokens,
        grad_gating,
        grad_router,
        gate_sum.astype(jnp.bfloat16),
        up_sum.astype(jnp.bfloat16),
        down_sum.astype(jnp.bfloat16),
        in_norms,
        down_norms,
        router_norms,
    )


def solution(mesh):
    split = Mesh(mesh.devices.reshape(8, 8, 2, mesh.shape["tp"]), ("ep_0", "ep_1", "ep_2", "tp"))
    in_specs = (
        P(EP, None),
        P(EP, None),
        P(EP, None),
        P(),
        P(EP, None, "tp"),
        P(EP, None, "tp"),
        P(EP, "tp", None),
    )
    out_specs = (
        P(EP, "tp"),
        P(EP, None),
        P(EP, None),
        P(EP, None, "tp"),
        P(EP, None, "tp"),
        P(EP, "tp", None),
        P(EP, None, None),
        P(EP, "tp"),
        P(EP),
    )
    return jax.shard_map(
        shards, mesh=split, in_specs=in_specs, out_specs=out_specs, check_vma=False
    )
```

profile of v0, /device:TPU:1, one launch (start us, length us, event | category | flops | bytes accessed | tf_op | source)
XLA Modules:
  0.0 282.2 jit_solution(13702238022662814079)
XLA Ops:
  7.2 0.7 broadcast_multiply_fusion
  8.0 0.8 copy.84
  8.9 0.1 eq.41
  9.4 0.2 fusion.13
  9.7 0.2 fusion.17
  9.9 1.4 scatter_custom_fusion
  11.4 1.0 pad_dynamic-slice_fusion
  12.4 2.0 gather_fusion.2
  14.5 2.0 gather_fusion.1
  16.6 0.5 pad_maximum_fusion
  17.1 49.2 %all_to_all.36 = bf16[128,8,512]{2,1,0:T(8,128)(2,1)S(1)} all-to-all(bf16[128,8,512]{2,1,0:T(8,128)(2,1)S(1)} %pad_maximum_fusion), channel_id=1, replica_groups=mesh['ep_0'=8,'ep_1'=8,'ep_2'=2,'tp'=4] {'ep_0','ep_1','ep_2'}, dimensions={0} | all-to-all | bytes 2097152 | tf_op jit(solution)/shard_map/all_to_all | solution.py:18
  66.3 0.3 fusion.39
  66.6 1.7 pad_maximum_fusion.1
  68.3 0.3 fusion.43
  68.6 0.3 fusion.22
  69.2 0.1 reshape.207
  69.4 3.5 %gather_fusion = f32[512]{0:T(512)S(1)} fusion(f32[257]{0:T(512)S(1)} %pad_maximum_fusion.4, s32[1024]{0:T(1024)S(1)} %get-tuple-element.95), kind=kCustom, calls=%fused_computation | custom fusion | bytes 6144 | tf_op jit(solution)/shard_map/gather | solution.py:121
  73.0 17.7 %all_to_all.37 = f32[128,1,4]{2,1,0:T(1,128)S(1)} all-to-all(f32[128,1,4]{2,1,0:T(1,128)S(1)} %bitcast.93), channel_id=1, replica_groups=mesh['ep_0'=8,'ep_1'=8,'ep_2'=2,'tp'=4] {'ep_0','ep_1','ep_2'}, dimensions={0} | all-to-all | bytes 4096 | tf_op jit(solution)/shard_map/all_to_all | solution.py:137
  90.7 0.5 broadcast.129
  91.2 0.8 reduce.17
  92.1 25.2 %all-gather.2.cloned.1.call-done = bf16[256,4,2048]{2,1,0:T(4,128)(2,1)} async-done(((bf16[256,4,512]{2,1,0:T(4,128)(2,1)}), bf16[256,4,2048]{2,1,0:T(4,128)(2,1)}) %all-gather.2.cloned.1.call-update) | async-done | bytes 4194320 | tf_op jit(solution)/shard_map/all_gather | solution.py:31
  117.3 5.4 %fusion.38 = (bf16[128,4,2048]{2,1,0:T(4,128)(2,1)S(1)}, bf16[128,4,2048]{2,1,0:T(4,128)(2,1)}) fusion(bf16[256,4,2048]{2,1,0:T(4,128)(2,1)} %all-gather.2.cloned.1.call-done), kind=kLoop, calls=%fused_computation.90 | loop fusion | bytes 8388608 | tf_op jit(solution)/shard_map/split | solution.py:31
  122.7 2.1 reshape.211
  124.7 2.5 reshape.213
  127.3 0.8 fusion.3
  128.1 0.2 copy-done.4
  128.3 0.8 fusion.6
  129.2 0.7 copy-done.1
  130.0 1.6 fusion.10
  131.6 1.3 convert_bitcast_fusion.2
  132.8 1.2 convert_bitcast_fusion.1
  134.1 8.0 %all_to_all.38 = f32[4,1,4608]{2,1,0:T(1,128)S(1)} all-to-all(f32[4,1,4608]{2,1,0:T(1,128)S(1)} %broadcast_in_dim.11), channel_id=1, replica_groups=mesh['ep_0'=8,'ep_1'=8,'ep_2'=2,'tp'=4] {'tp'}, dimensions={0} | all-to-all | bytes 147456 | tf_op jit(solution)/shard_map/all_to_all | solution.py:47
  142.2 0.7 slice.28
  142.9 17.1 %all-to-all-start.5 = ((f32[128,1,4]{2,1,0:T(1,128)}), f32[128,1,4]{2,1,0:T(1,128)S(1)}, u32[]{:S(2)}, u32[]{:S(2)}) async-start(f32[128,1,4]{2,1,0:T(1,128)} %bitcast.13), calls=%async_computation.5 | async-start | bytes 131072 | tf_op jit(solution)/shard_map/all_to_all | solution.py:182
  160.1 11.4 %all-to-all-done.5 = f32[128,1,4]{2,1,0:T(1,128)S(1)} async-done(((f32[128,1,4]{2,1,0:T(1,128)}), f32[128,1,4]{2,1,0:T(1,128)S(1)}, u32[]{:S(2)}, u32[]{:S(2)}) %all-to-all-start.5) | async-done | bytes 2080 | tf_op jit(solution)/shard_map/all_to_all | solution.py:182
  171.4 0.8 reduce.18
  172.4 1.9 gather_fusion.4
  174.6 0.1 copy.104
  174.7 0.3 fusion.21
  175.1 0.3 convolution_bitcast_fusion
  175.4 0.3 copy.97
  175.8 1.1 copy.98
  176.9 0.7 fusion.1
  177.7 0.3 copy-done.5
  178.0 0.7 add_convert_fusion
  178.7 2.8 reshape.216
  181.5 3.3 %copy.111 = bf16[1,512,4,512]{3,1,0,2:T(8,128)(2,1)} copy(bf16[1,512,4,512]{3,2,1,0:T(4,128)(2,1)} %reshape.216) | data formatting | bytes 4194304 | tf_op jit(solution)/shard_map/reshape | solution.py:36
  184.8 3.6 %all-to-all-start.2 = ((bf16[4,1,512,512]{3,2,1,0:T(8,128)(2,1)}), bf16[4,1,512,512]{3,2,1,0:T(8,128)(2,1)S(1)}, u32[]{:S(2)}, u32[]{:S(2)}) async-start(bf16[4,1,512,512]{3,2,1,0:T(8,128)(2,1)} %bitcast.88), calls=%async_computation.2 | async-start | bytes 4194304 | tf_op jit(solution)/shard_map/all_to_all | solution.py:41
  188.5 0.7 reduce-scatter.6.cloned.1.call-update
  189.1 24.8 %all-to-all-done.2 = bf16[4,1,512,512]{3,2,1,0:T(8,128)(2,1)S(1)} async-done(((bf16[4,1,512,512]{3,2,1,0:T(8,128)(2,1)}), bf16[4,1,512,512]{3,2,1,0:T(8,128)(2,1)S(1)}, u32[]{:S(2)}, u32[]{:S(2)}) %all-to-all-start.2) | async-done | bytes 2097184 | tf_op jit(solution)/shard_map/all_to_all | solution.py:41
  213.9 0.6 reduce_sum.109
  214.6 0.9 reshape_transpose_reshape.2
  215.5 7.1 %all-to-all-start.3 = ((bf16[128,4,512]{2,1,0:T(4,128)(2,1)}), bf16[128,4,512]{2,1,0:T(4,128)(2,1)S(1)}, u32[]{:S(2)}, u32[]{:S(2)}) async-start(bf16[128,4,512]{2,1,0:T(4,128)(2,1)} %reshape_transpose_reshape.2), calls=%async_computation.3 | async-start | bytes 1048576 | tf_op jit(solution)/shard_map/all_to_all | solution.py:179
  222.7 2.0 copy.101
  224.7 2.1 copy.100
  226.8 1.8 multiply_reduce_fusion
  228.6 0.6 pad_maximum_fusion.3
  229.2 14.1 %all-to-all-done.3 = bf16[128,4,512]{2,1,0:T(4,128)(2,1)S(1)} async-done(((bf16[128,4,512]{2,1,0:T(4,128)(2,1)}), bf16[128,4,512]{2,1,0:T(4,128)(2,1)S(1)}, u32[]{:S(2)}, u32[]{:S(2)}) %all-to-all-start.3) | async-done | bytes 524320 | tf_op jit(solution)/shard_map/all_to_all | solution.py:179
  243.4 1.2 gather_fusion.3
  244.6 0.3 reshape.221
  244.9 0.6 reduce_sum.110
  245.6 1.8 fusion
  247.4 26.9 %reduce-scatter.8.cloned.1.call-done = f32[1,16,128]{2,1,0:T(8,128)} async-done(((f32[8,16,128]{2,1,0:T(8,128)}), f32[1,16,128]{2,1,0:T(8,128)}) %reduce-scatter.8.cloned.1.call-update) | async-done | bytes 8208 | tf_op jit(solution)/shard_map/reduce_scatter | solution.py:69
  274.3 1.3 multiply_reduce_fusion.3
  (65 shorter events, 2.3 us)
Async XLA Ops:
  7.2 120.1 %copy-start = (bf16[1,2048,128]{2,1,0:T(8,128)(2,1)S(1)}, bf16[1,2048,128]{2,1,0:T(8,128)(2,1)}, u32[]{:S(2)}) copy-start(bf16[1,2048,128]{2,1,0:T(8,128)(2,1)} %param.11) | copy-start | bytes 1572868
  7.2 110.1 %all-gather.2.cloned.1.call-start = ((), (), s32[]{:S(2)}) async-start(), calls=%async_computation.9 | async-start | bytes 5242880 | tf_op jit(solution)/shard_map/all_gather | solution.py:31
  66.6 1.7 copy-start.3
  66.6 1.7 copy-start.6
  127.3 1.0 copy-start.4
  128.3 1.6 copy-start.1
  128.3 1.7 copy-start.11
  142.2 0.8 copy-start.8
  142.9 28.5 %all-to-all-start.5 = ((f32[128,1,4]{2,1,0:T(1,128)}), f32[128,1,4]{2,1,0:T(1,128)S(1)}, u32[]{:S(2)}, u32[]{:S(2)}) async-start(f32[128,1,4]{2,1,0:T(1,128)} %bitcast.13), calls=%async_computation.5 | async-start | bytes 131072 | tf_op jit(solution)/shard_map/all_to_all | solution.py:182
  160.0 28.4 %reduce-scatter.4.cloned.1.call-start = ((), (), s32[]{:S(2)}) async-start(), calls=%async_computation.10 | async-start | bytes 1572864 | tf_op jit(solution)/shard_map/reduce_scatter | solution.py:69
  174.5 1.2 copy-start.10
  176.9 1.0 copy-start.5
  184.8 29.1 %all-to-all-start.2 = ((bf16[4,1,512,512]{3,2,1,0:T(8,128)(2,1)}), bf16[4,1,512,512]{3,2,1,0:T(8,128)(2,1)S(1)}, u32[]{:S(2)}, u32[]{:S(2)}) async-start(bf16[4,1,512,512]{3,2,1,0:T(8,128)(2,1)} %bitcast.88), calls=%async_computation.2 | async-start | bytes 4194304 | tf_op jit(solution)/shard_map/all_to_all | solution.py:41
  188.4 57.2 %reduce-scatter.6.cloned.1.call-start = ((), (), s32[]{:S(2)}) async-start(), calls=%async_computation.11 | async-start | bytes 589824 | tf_op jit(solution)/shard_map/reduce_scatter | solution.py:69
  214.6 12.2 %copy-start.2 = (bf16[512,2048]{1,0:T(8,128)(2,1)S(1)}, bf16[512,2048]{1,0:T(8,128)(2,1)}, u32[]{:S(2)}) copy-start(bf16[512,2048]{1,0:T(8,128)(2,1)} %reshape.211) | copy-start | bytes 6291460
  214.6 12.2 %copy-start.7 = (bf16[512,128]{0,1:T(8,128)(2,1)S(1)}, bf16[512,128]{0,1:T(8,128)(2,1)}, u32[]{:S(2)}) copy-start(bf16[512,128]{0,1:T(8,128)(2,1)} %get-tuple-element.73) | copy-start | bytes 393220
  215.5 27.8 %all-to-all-start.3 = ((bf16[128,4,512]{2,1,0:T(4,128)(2,1)}), bf16[128,4,512]{2,1,0:T(4,128)(2,1)S(1)}, u32[]{:S(2)}, u32[]{:S(2)}) async-start(bf16[128,4,512]{2,1,0:T(4,128)(2,1)} %reshape_transpose_reshape.2), calls=%async_computation.3 | async-start | bytes 1048576 | tf_op jit(solution)/shard_map/all_to_all | solution.py:179
  222.6 51.7 %reduce-scatter.8.cloned.1.call-start = ((), (), s32[]{:S(2)}) async-start(), calls=%async_computation.12 | async-start | bytes 73728 | tf_op jit(solution)/shard_map/reduce_scatter | solution.py:69
  224.7 3.8 %copy-start.9 = (f32[4608]{0:T(1024)S(1)}, f32[4608]{0:T(1024)}, u32[]{:S(2)}) copy-start(f32[4608]{0:T(1024)} %copy-done.8) | copy-start | bytes 55300
Sparse Core Ops, SparseCore 0:
  68.4 48.8 all-gather.1
  177.0 8.0 reduce-scatter.3
  192.0 32.9 reduce-scatter.5
  245.7 28.5 reduce-scatter.7
where the time goes:
time: 288 us; the launch traced here: 282 us
  waiting for transfers between devices  103 us (36%)
  blocking collectives  74.9 us (26%)
  local copies, waits for them, and re-layouts  41.6 us (14%)
  starting transfers between devices  28 us (10%)
  between operations  14.2 us (5%)
  matrix products  12 us (4%)
  other arithmetic  8.36 us (3%)
    all_to_all x1, blocking collectives, side_by_side(): lax.all_to_all(both, axis, split_axis=split_dim, concat_axis=concat_dim,...  49.2 us
    reduce_scatter x3, waiting for transfers between devices, sum_in_order(): blocks = lax.psum_scatter(blocks, axes[k], scatter_dimension=0, tiled=True)  27 us
    all_gather x1, waiting for transfers between devices, side_by_side_2(): lax.all_gather(both, axis, axis=dim, tiled=True)  25.2 us
    all_to_all x1, waiting for transfers between devices, sum_at_owner(): lax.all_to_all(blocks, axis, split_axis=0, concat_axis=0, tiled=True)  24.8 us
    all_to_all x1, blocking collectives, shards(): lax.all_to_all(sent_gating, EP, split_axis=0, concat_axis=0, tiled=True)  17.7 us
    all_to_all x1, starting transfers between devices, shards(): lax.all_to_all(by_source(gating_total), EP, split_axis=0, concat_axis=0,...  17.1 us
    all_to_all x1, waiting for transfers between devices, shards(): lax.all_to_all(by_source(slot_values), EP, split_axis=0, concat_axis=0, t...  14.1 us
    all_to_all x1, waiting for transfers between devices, shards(): lax.all_to_all(by_source(gating_total), EP, split_axis=0, concat_axis=0,...  11.4 us
  transfers between devices with their start and end apart: 7, of which 5 were waited for; matrix products, arithmetic and copies ran while one was open for 9% of the time, Pallas kernels for 0%

commit v1 on v0

v1 whole, which is shorter than its diff:
```python
import functools

import jax
import jax.numpy as jnp
from jax import lax
from jax.experimental import pallas as pl
from jax.experimental.pallas import tpu as pltpu
from jax.sharding import Mesh
from jax.sharding import PartitionSpec as P

AXES = ("ep_0", "ep_1", "ep_2", "tp")
EP = AXES[:3]
MESH = pl.DeviceIdType.MESH
CAP = 4
LANES = 128
F32 = jnp.float32
BF16 = jnp.bfloat16
HIGH = lax.Precision.HIGHEST


class Sizes:
    def __init__(self, shape, tokens, width, hidden):
        self.nz, self.ny, self.nc, self.nx = shape
        self.nj = self.ny * self.nc
        self.ne = self.nz * self.nj
        self.t = tokens
        self.d = width
        self.f = hidden
        self.sl = width // self.nx
        self.fb = self.sl // LANES
        self.ur = CAP * self.fb
        self.gs = LANES // self.ur
        self.ng = self.ne // self.gs
        self.rows = self.gs * CAP
        self.s = self.ne * CAP
        self.zs = self.nj * CAP
        near = []
        for step in range(1, self.nz // 2 + 1):
            near += [step] if 2 * step == self.nz else [step, self.nz - step]
        self.near = near


def iota(shape, dim):
    return lax.broadcasted_iota(jnp.int32, shape, dim)


def dot(a, b, dims=((1,), (0,)), precision=None):
    return lax.dot_general(a, b, (dims, ((), ())), precision=precision, preferred_element_type=F32)


def to_unit(n):
    u, l = iota((LANES, LANES), 0), iota((LANES, LANES), 1)
    dev, fb, i = u // n.ur, (u // CAP) % n.fb, u % CAP
    return jnp.where(l == fb * n.rows + dev * CAP + i, 1.0, 0.0).astype(BF16)


def to_linear(n):
    u, l = iota((LANES, LANES), 1), iota((LANES, LANES), 0)
    dev, fb, i = u // n.ur, (u // CAP) % n.fb, u % CAP
    return jnp.where(l == fb * n.rows + dev * CAP + i, 1.0, 0.0).astype(BF16)


def stacked(n, block):
    return jnp.concatenate([block[:, b * LANES : (b + 1) * LANES] for b in range(n.fb)], axis=0)


def place(n):
    z, y = lax.axis_index(AXES[0]), lax.axis_index(AXES[1])
    c, x = lax.axis_index(AXES[2]), lax.axis_index(AXES[3])
    return z, y * n.nc + c, x


def wrap(value, size):
    return lax.rem(value, size)


def at_z(z):
    return {AXES[0]: z}


def at_j(n, j):
    return {AXES[1]: j // n.nc, AXES[2]: lax.rem(j, n.nc)}


def at_x(x):
    return {AXES[3]: x}


def greet(n):
    z, j, x = place(n)
    barrier = pltpu.get_barrier_semaphore()

    def tell(device):
        pl.semaphore_signal(barrier, inc=1, device_id=device, device_id_type=MESH)

    for dz in range(1, n.nz):
        tell(at_z(wrap(z + dz, n.nz)))

    @pl.loop(1, n.nj)
    def _(dj):
        tell(at_j(n, wrap(j + dj, n.nj)))

    for dx in range(1, n.nx):
        tell(at_x(wrap(x + dx, n.nx)))
    pl.semaphore_wait(barrier, n.nz + n.nj + n.nx - 3)


def remote(src, dst, send_sem, recv_sem, device):
    return pltpu.make_async_remote_copy(
        src_ref=src,
        dst_ref=dst,
        send_sem=send_sem,
        recv_sem=recv_sem,
        device_id=device,
        device_id_type=MESH,
    )


def wait_bytes(ref, sem):
    pltpu.make_async_copy(ref, ref, sem).wait()


def prepare(n, x, tok_ref, cot_ref, rout_ref, rw_ref, x_ref, g_ref, meta_ref):
    logits = dot(tok_ref[...], rw_ref[...])
    eio = iota((n.t, n.ne), 1)
    r0, r1 = rout_ref[:, 0:1], rout_ref[:, 1:2]
    oh0, oh1 = eio == r0, eio == r1
    s0 = jax.nn.sigmoid(jnp.sum(jnp.where(oh0, logits, 0.0), axis=1, keepdims=True))
    s1 = jax.nn.sigmoid(jnp.sum(jnp.where(oh1, logits, 0.0), axis=1, keepdims=True))
    total = s0 + s1
    g0, g1 = s0 / total, s1 / total
    f0, f1 = jnp.where(oh0, 1.0, 0.0), jnp.where(oh1, 1.0, 0.0)
    a, b = iota((n.t, n.t), 0), iota((n.t, n.t), 1)
    before = jnp.where(b < a, 1.0, 0.0).astype(BF16)
    c0 = dot(before, f0.astype(BF16))
    c1 = dot(before, f1.astype(BF16)) + jnp.sum(f0, axis=0, keepdims=True)
    w0 = jnp.sum(f0 * c0, axis=1, keepdims=True)
    w1 = jnp.sum(f1 * c1, axis=1, keepdims=True)
    r0f, r1f = r0.astype(F32), r1.astype(F32)
    columns = (r0f, r1f, w0, w1, g0, g1, s0, s1, total)
    lane = iota((n.t, LANES), 1)
    meta = jnp.zeros((n.t, LANES), F32)
    for k, column in enumerate(columns):
        meta = jnp.where(lane == k, column, meta)
    meta_ref[...] = meta
    lanef = lane.astype(F32)
    g_all = dot(f0, jnp.where(lanef == w0, g0, 0.0), ((0,), (0,)), HIGH) + dot(
        f1, jnp.where(lanef == w1, g1, 0.0), ((0,), (0,)), HIGH
    )
    for e in range(n.ne):
        g_ref[e] = g_all[e : e + 1, :]
    eye = a == b
    row0 = jnp.sum(jnp.where(eye, r0f * CAP + w0, 0.0), axis=0, keepdims=True)
    row1 = jnp.sum(jnp.where(eye, r1f * CAP + w1, 0.0), axis=0, keepdims=True)
    sio = iota((n.s, n.t), 0).astype(F32)
    pick = jnp.where((sio == row0) | (sio == row1), 1.0, 0.0).astype(BF16)
    unit = to_unit(n)
    mine = pl.ds(pl.multiple_of(x * n.sl, LANES), n.sl)
    for k, ref in enumerate((tok_ref, cot_ref)):
        lin = dot(pick, ref[:, mine]).astype(BF16)
        for g in range(n.ng):
            block = stacked(n, lin[g * n.rows : (g + 1) * n.rows, :])
            moved = dot(unit, block).astype(BF16)
            x_ref[g * n.gs : (g + 1) * n.gs, :, k * LANES : (k + 1) * LANES] = moved.reshape(
                n.gs, n.ur, LANES
            )


def dispatch_kernel(
    n, tok_ref, cot_ref, rout_ref, rw_ref,
    rt_ref, gt_ref, meta_ref,
    x_ref, g_ref, r_ref, gr_ref,
    zs, zr, gzs, gzr, ys, yr, gys, gyr, ls, gls, xs, xr, fs, fr,
):
    z, j, x = place(n)
    greet(n)
    prepare(n, x, tok_ref, cot_ref, rout_ref, rw_ref, x_ref, g_ref, meta_ref)
    right, left = wrap(x + 1, n.nx), wrap(x + n.nx - 1, n.nx)
    half = n.nj // 2

    def z_copies(dz):
        to = wrap(z + dz, n.nz)
        block = pl.ds(to * n.nj, n.nj)
        return (
            remote(x_ref.at[block], r_ref.at[dz], zs.at[dz], zr.at[dz], at_z(to)),
            remote(g_ref.at[block], gr_ref.at[dz], gzs.at[dz], gzr.at[dz], at_z(to)),
        )

    for dz in n.near:
        for copy in z_copies(dz):
            copy.start()

    def source(dz):
        return wrap(z + n.nz - dz, n.nz)

    def unit_of(dz, unit):
        if dz == 0:
            return x_ref.at[z * n.nj + unit], g_ref.at[z * n.nj + unit]
        return r_ref.at[dz, unit], gr_ref.at[dz, unit]

    def local_copies(dz):
        own, gown = unit_of(dz, j)
        to = source(dz) * n.nj + j
        return (
            pltpu.make_async_copy(own, rt_ref.at[x, to], ls.at[dz]),
            pltpu.make_async_copy(gown, gt_ref.at[to], gls.at[dz]),
        )

    def y_stage(dz):
        if dz:
            for copy in z_copies(dz):
                copy.wait_recv()
        for copy in local_copies(dz):
            copy.start()
        to = source(dz) * n.nj + j

        @pl.loop(1, n.nj)
        def _(dj):
            other = wrap(j + dj, n.nj)
            unit, gunit = unit_of(dz, other)
            remote(unit, rt_ref.at[x, to], ys.at[dz], yr.at[dz], at_j(n, other)).start()
            remote(gunit, gt_ref.at[to], gys.at[dz], gyr.at[dz], at_j(n, other)).start()

    def chunk(dz, owner, first, count):
        return rt_ref.at[owner, pl.ds(source(dz) * n.nj + first, count)]

    def x_copies(dz):
        own = chunk(dz, x, 0, n.nj)
        return (
            remote(own, own, xs.at[0, dz], xr.at[0, dz], at_x(right)),
            remote(own, own, xs.at[1, dz], xr.at[1, dz], at_x(left)),
        )

    def x_stage(dz):
        for copy in local_copies(dz):
            copy.wait()
        wait_bytes(chunk(dz, x, 0, n.nj - 1), yr.at[dz])
        wait_bytes(gt_ref.at[pl.ds(0, n.nj - 1)], gyr.at[dz])
        for copy in x_copies(dz):
            copy.start()

    def forward_copies(dz):
        one, two = chunk(dz, left, 0, half), chunk(dz, right, half, n.nj - half)
        return (
            remote(one, one, fs.at[0, dz], fr.at[0, dz], at_x(right)),
            remote(two, two, fs.at[1, dz], fr.at[1, dz], at_x(left)),
        )

    def f_stage(dz):
        for copy, forward in zip(x_copies(dz), forward_copies(dz)):
            copy.wait_recv()
            forward.start()

    def done(dz):
        for copy in forward_copies(dz):
            copy.wait_recv()

    order = [0] + n.near
    stages = (y_stage, x_stage, f_stage, done)
    for step in range(n.nz + len(stages) - 1):
        for k, stage in enumerate(stages):
            if 0 <= step - k < n.nz:
                stage(order[step - k])
    for dz in order:
        if dz:
            for copy in z_copies(dz):
                copy.wait_send()
        wait_bytes(chunk(dz, x, 0, n.nj - 1), ys.at[dz])
        wait_bytes(gt_ref.at[pl.ds(0, n.nj - 1)], gys.at[dz])
        for copy in (*x_copies(dz), *forward_copies(dz)):
            copy.wait_send()


def dma(*shape):
    return pltpu.SemaphoreType.DMA(shape)


def vmem(*_):
    return pl.BlockSpec(memory_space=pltpu.VMEM)


def dispatch(n, tokens, cotangent, routing, router_weight):
    return pl.pallas_call(
        functools.partial(dispatch_kernel, n),
        name="dispatch",
        out_shape=(
            jax.ShapeDtypeStruct((n.nx, n.ne, n.ur, 2 * LANES), BF16),
            jax.ShapeDtypeStruct((n.ne, 1, LANES), F32),
            jax.ShapeDtypeStruct((n.t, LANES), F32),
        ),
        in_specs=[vmem()] * 4,
        out_specs=(vmem(), vmem(), vmem()),
        scratch_shapes=[
            pltpu.VMEM((n.ne, n.ur, 2 * LANES), BF16),
            pltpu.VMEM((n.ne, 1, LANES), F32),
            pltpu.VMEM((n.nz, n.nj, n.ur, 2 * LANES), BF16),
            pltpu.VMEM((n.nz, n.nj, 1, LANES), F32),
            *([dma(n.nz)] * 10),
            *([dma(2, n.nz)] * 4),
        ],
        compiler_params=pltpu.CompilerParams(collective_id=0, has_side_effects=True),
    )(tokens, cotangent, routing, router_weight)


def expert_kernel(
    n, rt_ref, gt_ref, wg_ref, wu_ref, wd_ref,
    gg_ref, gu_ref, gd_ref, dn_ref, back_ref, gp_ref, nrm_ref,
    rows_ref, cots_ref, w_ref,
):
    hid = n.f
    lin = to_linear(n)

    @pl.loop(0, n.ng)
    def _(g):
        at = pl.ds(pl.multiple_of(g * n.rows, n.rows), n.rows)
        for k in range(n.nx):
            block = rt_ref[k, pl.ds(g * n.gs, n.gs)].reshape(LANES, 2 * LANES)
            moved = dot(lin, block).astype(BF16)
            for b in range(n.fb):
                part = moved[b * n.rows : (b + 1) * n.rows]
                lanes = pl.ds(k * n.sl + b * LANES, LANES)
                rows_ref[at, lanes] = part[:, :LANES]
                cots_ref[at, lanes] = part[:, LANES:]

    w_ref[:, :hid] = wg_ref[...]
    w_ref[:, hid:] = wu_ref[...]
    owner = iota((n.s, n.ne), 0) // CAP == iota((n.s, n.ne), 1)
    spread = dot(jnp.where(owner, 1.0, 0.0), gt_ref[:, 0, :], precision=HIGH)
    slot = iota((n.s, LANES), 0) % CAP == iota((n.s, LANES), 1)
    gating = jnp.sum(jnp.where(slot, spread, 0.0), axis=1, keepdims=True)

    rows, cots = rows_ref[...], cots_ref[...]
    pre = dot(rows, w_ref[...])
    pre_gate, pre_up = pre[:, :hid], pre[:, hid:]
    sig = jax.nn.sigmoid(pre_gate)
    activated = pre_gate * sig
    slope = sig * (1.0 + pre_gate * (1.0 - sig))
    hidden = (activated * pre_up).astype(BF16)
    back = dot(cots, wd_ref[...], ((1,), (1,)))
    wide = hidden.astype(F32)
    gp_ref[...] = dot(jnp.ones((8, hid), F32), wide * back, ((1,), (1,)), HIGH)
    scaled = gating * back
    grads = jnp.concatenate(
        [(scaled * pre_up * slope).astype(BF16), (scaled * activated).astype(BF16)], axis=1
    )
    scaled_hidden = (gating * wide).astype(BF16)
    back_ref[...] = dot(grads, w_ref[...], ((1,), (1,))).astype(BF16)
    both = dot(grads, rows, ((0,), (0,)))
    for k, ref in enumerate((gg_ref, gu_ref)):
        part = both[k * hid : (k + 1) * hid, :]
        nrm_ref[k : k + 1, :] = jnp.sum(part * part, axis=0, keepdims=True)
        ref[...] = part.T.astype(BF16)
    down = dot(scaled_hidden, cots, ((0,), (0,)))
    gd_ref[...] = down.astype(BF16)
    squares = jnp.sum(down * down, axis=1, keepdims=True)
    eye = iota((hid, hid), 0) == iota((hid, hid), 1)
    dn_ref[...] = jnp.sum(jnp.where(eye, squares, 0.0), axis=0, keepdims=True)


def experts(n, rt, gt, wg, wu, wd):
    def like(shape, dtype):
        return jax.ShapeDtypeStruct(shape, dtype)

    return pl.pallas_call(
        functools.partial(expert_kernel, n),
        name="experts",
        out_shape=(
            like((n.d, n.f), BF16),
            like((n.d, n.f), BF16),
            like((n.f, n.d), BF16),
            like((1, n.f), F32),
            like((n.s, n.d), BF16),
            like((8, n.s), F32),
            like((2, n.d), F32),
        ),
        in_specs=[vmem()] * 5,
        out_specs=tuple([vmem()] * 7),
        scratch_shapes=[
            pltpu.VMEM((n.s, n.d), BF16),
            pltpu.VMEM((n.s, n.d), BF16),
            pltpu.VMEM((n.d, 2 * n.f), BF16),
        ],
        compiler_params=pltpu.CompilerParams(vmem_limit_bytes=60 * 1024 * 1024),
    )(rt, gt, wg, wu, wd)


def return_kernel(
    n, back_ref, gp_ref, nrm_ref, meta_ref, tok_ref, rw_ref,
    gt_out, gg_out, gr_out, in_out, rn_out,
    gall_ref, nall_ref, rv_ref, y_ref, rz_ref, v_ref,
    h_ref, hz_ref, hv_ref, q_ref, qz_ref, qy_ref, qv_ref, u_ref,
    xgs, xgr, xns, xnr, xvs, xvr, zvs, zvr, yvs, yvr, lvs,
    zgs, zgr, ygs, ygr, lgs, zqs, zqr, yqs, yqr, xqs, xqr,
):
    z, j, x = place(n)
    others = range(1, n.nx)
    far = n.near[::-1] + [0]
    greet(n)

    def sink(dz):
        return wrap(z + dz, n.nz)

    def source(dz):
        return wrap(z + n.nz - dz, n.nz)

    gall_ref[x] = gp_ref[0:1, :]
    nall_ref[x] = nrm_ref[...]

    def xg_copy(dx):
        to = wrap(x + dx, n.nx)
        return remote(gall_ref.at[x], gall_ref.at[x], xgs.at[dx], xgr.at[dx], at_x(to))

    def xn_copy(dx):
        to = wrap(x + dx, n.nx)
        return remote(nall_ref.at[x], nall_ref.at[x], xns.at[dx], xnr.at[dx], at_x(to))

    def rows_of(dz):
        return pl.ds(pl.multiple_of(sink(dz) * n.zs, n.zs), n.zs)

    def xv_copy(dz, dx):
        to = wrap(x + dx, n.nx)
        lanes = pl.ds(pl.multiple_of(to * n.sl, LANES), n.sl)
        return remote(
            back_ref.at[rows_of(dz), lanes], rv_ref.at[dx, dz],
            xvs.at[dx, dz], xvr.at[dx, dz], at_x(to),
        )

    for dx in others:
        xg_copy(dx).start()
    for dz in far:
        for dx in others:
            xv_copy(dz, dx).start()
    for dx in others:
        xn_copy(dx).start()

    def gate_home():
        for dx in others:
            xg_copy(dx).wait_recv()
        total = gall_ref[0]
        for k in others:
            total = total + gall_ref[k]
        keep = iota((n.ne, n.s), 1) // CAP == iota((n.ne, n.s), 0)
        lanes = iota((n.s, LANES), 0) % CAP == iota((n.s, LANES), 1)
        units = dot(
            jnp.where(keep, total, 0.0), jnp.where(lanes, 1.0, 0.0), precision=HIGH
        )
        for e in range(n.ne):
            h_ref[e] = units[e : e + 1, :]
        for dz in n.near:
            zg_copy(dz).start()

    def zg_copy(dz):
        block = pl.ds(sink(dz) * n.nj, n.nj)
        return remote(h_ref.at[block], hz_ref.at[dz], zgs.at[dz], zgr.at[dz], at_z(sink(dz)))

    def gate_unit(dz, unit):
        return h_ref.at[z * n.nj + unit] if dz == 0 else hz_ref.at[dz, unit]

    def gate_local(dz):
        return pltpu.make_async_copy(
            gate_unit(dz, j), hv_ref.at[source(dz) * n.nj + j], lgs.at[dz]
        )

    def gate_y():
        for dz in [0] + n.near:
            if dz:
                zg_copy(dz).wait_recv()
            gate_local(dz).start()
            to = source(dz) * n.nj + j

            @pl.loop(1, n.nj)
            def _(dj):
                other = wrap(j + dj, n.nj)
                remote(
                    gate_unit(dz, other), hv_ref.at[to], ygs.at[dz], ygr.at[dz], at_j(n, other)
                ).start()

    meta = meta_ref[...]

    def column(k):
        return meta[:, k : k + 1]

    eio = iota((n.t, n.ne), 1).astype(F32)
    oh0, oh1 = eio == column(0), eio == column(1)

    def gate_final():
        for dz in range(n.nz):
            gate_local(dz).wait()
            wait_bytes(hv_ref.at[pl.ds(0, n.nj - 1)], ygr.at[dz])
        home = hv_ref[:, 0, :]
        lanef = iota((n.t, LANES), 1).astype(F32)
        parts = []
        for oh, within in ((oh0, column(2)), (oh1, column(3))):
            got = dot(jnp.where(oh, 1.0, 0.0), home, precision=HIGH)
            parts.append(jnp.sum(jnp.where(lanef == within, got, 0.0), axis=1, keepdims=True))
        gg0, gg1 = parts
        k2 = iota((n.t, 2), 1)
        gg_out[...] = jnp.where(k2 == 0, gg0, gg1)
        weighted = column(4) * gg0 + column(5) * gg1
        s0, s1, total = column(6), column(7), column(8)
        c0 = (gg0 - weighted) / total * s0 * (1.0 - s0)
        c1 = (gg1 - weighted) / total * s1 * (1.0 - s1)
        return (jnp.where(oh0, c0, 0.0) + jnp.where(oh1, c1, 0.0)).astype(BF16)

    part_rows = n.d // n.ne
    quarter = part_rows // n.nx

    def zq_copy(dz):
        return remote(q_ref.at[sink(dz)], qz_ref.at[dz], zqs.at[dz], zqr.at[dz], at_z(sink(dz)))

    def router_z(grad_logits):
        full = dot(tok_ref[...], grad_logits, ((0,), (0,)))
        full = full.reshape(n.ne, part_rows, n.ne)
        mine = full[:, :quarter, :]
        for k in others:
            mine = jnp.where(x == k, full[:, k * quarter : (k + 1) * quarter, :], mine)
        q_ref[...] = mine.reshape(n.nz, n.nj, quarter, n.ne)
        for dz in n.near:
            zq_copy(dz).start()

    def yq_copy(dj):
        to = wrap(j + dj, n.nj)
        return remote(u_ref.at[to], qy_ref.at[dj], yqs, yqr, at_j(n, to))

    def router_y():
        total = q_ref[z]
        for dz in n.near:
            zq_copy(dz).wait_recv()
            total = total + qz_ref[dz]
        u_ref[...] = total

        @pl.loop(1, n.nj)
        def _(dj):
            yq_copy(dj).start()

    def xq_copy(dx):
        to = wrap(x + dx, n.nx)
        return remote(qv_ref.at[x], qv_ref.at[x], xqs.at[dx], xqr.at[dx], at_x(to))

    def router_x():
        wait_bytes(qy_ref.at[pl.ds(1, n.nj - 1)], yqr)
        total = u_ref[j]
        for dj in range(1, n.nj):
            total = total + qy_ref[dj]
        qv_ref[x] = total
        for dx in others:
            xq_copy(dx).start()

    def router_final():
        for dx in others:
            xq_copy(dx).wait_recv()
        for k in range(n.nx):
            block = qv_ref[k]
            gr_out[k * quarter : (k + 1) * quarter, :] = block
            square = jnp.sum(block * block, axis=1, keepdims=True)
            rn_out[k * quarter : (k + 1) * quarter, :] = jnp.broadcast_to(square, block.shape)

    unit = to_unit(n)

    def zv_copy(dz):
        return remote(y_ref.at[dz], rz_ref.at[dz], zvs.at[dz], zvr.at[dz], at_z(sink(dz)))

    def values_z(dz):
        own = pl.ds(pl.multiple_of(x * n.sl, LANES), n.sl)
        total = back_ref[rows_of(dz), own].astype(F32)
        for dx in others:
            xv_copy(dz, dx).wait_recv()
            total = total + rv_ref[dx, dz].astype(F32)
        total = total.astype(BF16)
        for g in range(n.zs // n.rows):
            moved = dot(unit, stacked(n, total[g * n.rows : (g + 1) * n.rows])).astype(BF16)
            y_ref[dz, g * n.gs : (g + 1) * n.gs] = moved.reshape(n.gs, n.ur, LANES)
        if dz:
            zv_copy(dz).start()

    def value_unit(dz, which):
        return y_ref.at[0, which] if dz == 0 else rz_ref.at[dz, which]

    def value_local(dz):
        return pltpu.make_async_copy(
            value_unit(dz, j), v_ref.at[source(dz) * n.nj + j], lvs.at[dz]
        )

    def values_y(dz):
        if dz:
            zv_copy(dz).wait_recv()
        value_local(dz).start()
        to = source(dz) * n.nj + j

        @pl.loop(1, n.nj)
        def _(dj):
            other = wrap(j + dj, n.nj)
            remote(
                value_unit(dz, other), v_ref.at[to], yvs.at[dz], yvr.at[dz], at_j(n, other)
            ).start()

    gate_home()
    grad_logits = None
    for step in range(n.nz + 1):
        if step < n.nz:
            values_z(far[step])
        if step:
            values_y(far[step - 1])
        if step == 0:
            gate_y()
        if step == 2 * n.nz // 8:
            grad_logits = gate_final()
            router_z(grad_logits)
        if step == 4 * n.nz // 8:
            router_y()
        if step == 6 * n.nz // 8:
            router_x()
    for dx in others:
        xn_copy(dx).wait_recv()
    total = nall_ref[0]
    for k in others:
        total = total + nall_ref[k]
    in_out[...] = total
    router_term = dot(
        grad_logits, rw_ref[pl.ds(pl.multiple_of(x * n.sl, n.sl), n.sl), :], ((1,), (1,))
    )
    router_final()
    for dz in range(n.nz):
        value_local(dz).wait()
        wait_bytes(v_ref.at[pl.ds(0, n.nj - 1)], yvr.at[dz])
    lin = to_linear(n)
    slots = []
    for g in range(n.ng):
        moved = dot(lin, v_ref[g * n.gs : (g + 1) * n.gs].reshape(LANES, LANES)).astype(BF16)
        slots.append(
            jnp.concatenate(
                [moved[b * n.rows : (b + 1) * n.rows] for b in range(n.fb)], axis=1
            )
        )
    slots = jnp.concatenate(slots, axis=0)
    sio = iota((n.t, n.s), 1).astype(F32)
    slot0, slot1 = column(0) * CAP + column(2), column(1) * CAP + column(3)
    pick = jnp.where((sio == slot0) | (sio == slot1), 1.0, 0.0).astype(BF16)
    gt_out[...] = (dot(pick, slots) + router_term).astype(BF16)

    for dx in others:
        for copy in (xg_copy(dx), xn_copy(dx), xq_copy(dx)):
            copy.wait_send()
        for dz in range(n.nz):
            xv_copy(dz, dx).wait_send()
    for dz in range(n.nz):
        if dz:
            for copy in (zg_copy(dz), zq_copy(dz), zv_copy(dz)):
                copy.wait_send()
        wait_bytes(hv_ref.at[pl.ds(0, n.nj - 1)], ygs.at[dz])
        wait_bytes(v_ref.at[pl.ds(0, n.nj - 1)], yvs.at[dz])
    wait_bytes(qy_ref.at[pl.ds(1, n.nj - 1)], yqs)


def back_home(n, back, gp, nrm, meta, tokens, router_weight):
    part_rows = n.d // n.ne
    quarter = part_rows // n.nx

    def like(shape, dtype):
        return jax.ShapeDtypeStruct(shape, dtype)

    return pl.pallas_call(
        functools.partial(return_kernel, n),
        name="back_home",
        out_shape=(
            like((n.t, n.sl), BF16),
            like((n.t, 2), F32),
            like((part_rows, n.ne), F32),
            like((2, n.d), F32),
            like((part_rows, n.ne), F32),
        ),
        in_specs=[vmem()] * 6,
        out_specs=tuple([vmem()] * 5),
        scratch_shapes=[
            pltpu.VMEM((n.nx, 1, n.s), F32),
            pltpu.VMEM((n.nx, 2, n.d), F32),
            pltpu.VMEM((n.nx, n.nz, n.zs, n.sl), BF16),
            pltpu.VMEM((n.nz, n.nj, n.ur, LANES), BF16),
            pltpu.VMEM((n.nz, n.nj, n.ur, LANES), BF16),
            pltpu.VMEM((n.ne, n.ur, LANES), BF16),
            pltpu.VMEM((n.ne, 1, LANES), F32),
            pltpu.VMEM((n.nz, n.nj, 1, LANES), F32),
            pltpu.VMEM((n.ne, 1, LANES), F32),
            pltpu.VMEM((n.nz, n.nj, quarter, n.ne), F32),
            pltpu.VMEM((n.nz, n.nj, quarter, n.ne), F32),
            pltpu.VMEM((n.nj, quarter, n.ne), F32),
            pltpu.VMEM((n.nx, quarter, n.ne), F32),
            pltpu.VMEM((n.nj, quarter, n.ne), F32),
            *([dma(n.nx)] * 4),
            *([dma(n.nx, n.nz)] * 2),
            *([dma(n.nz)] * 5),
            *([dma(n.nz)] * 7),
            pltpu.SemaphoreType.DMA,
            pltpu.SemaphoreType.DMA,
            *([dma(n.nx)] * 2),
        ],
        compiler_params=pltpu.CompilerParams(collective_id=1, has_side_effects=True),
    )(back, gp, nrm, meta, tokens, router_weight)


def shards(shape, tokens, cotangent, routing, router_weight, gate_weight, up_weight, down_weight):
    n = Sizes(shape, tokens.shape[0], tokens.shape[1], gate_weight.shape[2])
    rt, gt, meta = dispatch(n, tokens, cotangent, routing, router_weight)
    grad_gate, grad_up, grad_down, down_norms, back, gp, nrm = experts(
        n, rt, gt, gate_weight[0], up_weight[0], down_weight[0]
    )
    grad_tokens, grad_gating, grad_router, in_norms, router_norms = back_home(
        n, back, gp, nrm, meta, tokens, router_weight
    )
    return (
        grad_tokens,
        grad_gating,
        grad_router,
        grad_gate[None],
        grad_up[None],
        grad_down[None],
        in_norms[None],
        down_norms,
        router_norms[:, 0],
    )


def solution(mesh, shape=(8, 8, 2)):
    shape = (*shape, mesh.shape["tp"])
    split = Mesh(mesh.devices.reshape(shape), AXES)
    in_specs = (
        P(EP, None),
        P(EP, None),
        P(EP, None),
        P(),
        P(EP, None, "tp"),
        P(EP, None, "tp"),
        P(EP, "tp", None),
    )
    out_specs = (
        P(EP, "tp"),
        P(EP, None),
        P(EP, None),
        P(EP, None, "tp"),
        P(EP, None, "tp"),
        P(EP, "tp", None),
        P(EP, None, None),
        P(EP, "tp"),
        P(EP),
    )
    return jax.shard_map(
        functools.partial(shards, shape),
        mesh=split,
        in_specs=in_specs,
        out_specs=out_specs,
        check_vma=False,
    )
```

time: 288 us -> 142 us (0.49); the launches traced: 282 us -> 142 us
  Pallas kernels: 0 us -> 133 us
  waiting for transfers between devices: 103 us -> 0 us
  blocking collectives: 74.9 us -> 0 us
  local copies, waits for them, and re-layouts: 41.6 us -> 8.4 us
  starting transfers between devices: 28 us -> 0 us
  between operations: 14.2 us -> 0.66 us
  matrix products: 12 us -> 0 us
  other arithmetic: 8.36 us -> 0 us
    pallas_call x0 -> x3, Pallas kernels: none -> 133 us  [the longest x1 69 us: dispatch(): pl.pallas_call(functools.partial(dispatch_kernel, n), name='dispatch', ou...]
    all_to_all x3 -> x0, blocking collectives: 74.9 us -> none  [the longest x1 49.2 us: side_by_side(): lax.all_to_all(both, axis, split_axis=split_dim, concat_axis=concat_dim,...]
    all_to_all x3 -> x0, waiting for transfers between devices: 50.3 us -> none  [the longest x1 24.8 us: sum_at_owner(): lax.all_to_all(blocks, axis, split_axis=0, concat_axis=0, tiled=True)]
    all_to_all x3 -> x0, starting transfers between devices: 27.8 us -> none  [the longest x1 17.1 us: shards(): lax.all_to_all(by_source(gating_total), EP, split_axis=0, concat_axis=0,...]
    reduce_scatter x3 -> x0, waiting for transfers between devices: 27 us -> none  [sum_in_order(): blocks = lax.psum_scatter(blocks, axes[k], scatter_dimension=0, tiled=True)]
    all_gather x1 -> x0, waiting for transfers between devices: 25.2 us -> none  [side_by_side_2(): lax.all_gather(both, axis, axis=dim, tiled=True)]
    dot_general x13 -> x0, matrix products: 12 us -> none  [the longest x1 1.76 us: shards(): jnp.einsum('te,de->td', grad_logits, router_slice, preferred_element_type...]
    gather x5 -> x0, local copies, waits for them, and re-layouts: 10.5 us -> none  [the longest x1 3.49 us: shards(): sent_gating = padded_gating[assignment].reshape(experts_all, capacity)]
  transfers between devices with their start and end apart: 7 -> 0, of which waited for: 5 -> 0; matrix products, arithmetic and copies ran while one was open for 9% -> 0% of each run, Pallas kernels for 0% -> 0%
where the time goes in v1:
time: 142 us
  Pallas kernels  133 us (94%)
  local copies, waits for them, and re-layouts  8.4 us (6%)
    pallas_call x1, Pallas kernels, dispatch(): pl.pallas_call(functools.partial(dispatch_kernel, n), name='dispatch', ou...  69 us
    pallas_call x1, Pallas kernels, back_home(): pl.pallas_call(functools.partial(return_kernel, n), name='back_home', out...  52 us
    pallas_call x1, Pallas kernels, experts(): pl.pallas_call(functools.partial(expert_kernel, n), name='experts', out_s...  11.6 us
    unnamed x5, local copies, waits for them, and re-layouts  7.07 us

profile of v1, /device:TPU:1, one launch (start us, length us, event | category | flops | bytes accessed | tf_op | source)
XLA Modules:
  0.0 141.6 jit_solution(1094361333120374492)
XLA Ops:
  0.6 1.4 copy.18.rout_ref
  2.1 69.0 %dispatch.1 = (bf16[4,128,16,256]{3,2,1,0:T(8,128)(2,1)}, f32[128,1,128]{2,1,0:T(1,128)}, f32[128,128]{1,0:T(8,128)}) custom-call(bf16[128,2048]{1,0:T(8,128)(2,1)} %tok_ref.3, bf16[128,2048]{1,0:T(8,128)(2,1)} %cot_ref.1, s32[128,2]{1,0:T(8,128)} %copy.18.rout_ref, bf16[2048,128]{1,0:T(8,128)(2,1)} %rw_ref.3), custom_call_target="tpu_custom_call" | custom-call | tf_op jit(solution)/shard_map/dispatch/pallas_call | solution.py:283
  71.0 11.6 %experts.1 = (bf16[2048,128]{1,0:T(8,128)(2,1)}, bf16[2048,128]{1,0:T(8,128)(2,1)}, bf16[128,2048]{1,0:T(8,128)(2,1)}, f32[1,128]{1,0:T(1,128)}, bf16[512,2048]{...) custom-call(bf16[4,128,16,256]{3,2,1,0:T(8,128)(2,1)} %get-tuple-element.24.rt_ref, ...), custom_call_target="tpu_custom_call" | custom-call | tf_op jit(solution)/shard_map/experts/pallas_call | solution.py:364
  82.6 52.0 %back_home.1 = (bf16[128,512]{1,0:T(8,128)(2,1)}, f32[128,2]{1,0:T(8,128)}, f32[16,128]{1,0:T(8,128)}, f32[2,2048]{1,0:T(2,128)}, f32[16,128]{1,0:T(8,128)}) custom-call(bf16[512,2048]{1,0:T(8,128)(2,1)} %get-tuple-element.26.back_ref, f32[8,512]{1,0:T(8,128)} %get-tuple-element.27.gp_ref, f32[2,2048]{1,0:T(2,128)} %get-tuple-element.28.nrm_ref, ...), custom_call_target="tpu_custom_call" | custom-call | tf_op jit(solution)/shard_map/back_home/pallas_call | solution.py:662
  134.6 1.3 slice_reduce_fusion
  135.9 1.5 %copy.19 = f32[128,2]{0,1:T(2,128)} copy(f32[128,2]{1,0:T(8,128)} %get-tuple-element.49) | data formatting | bytes 2048
  137.4 1.6 %copy.23 = bf16[128,512]{1,0:T(8,128)(2,1)} copy(bf16[128,512]{1,0:T(8,128)(2,1)} %get-tuple-element.66) | data formatting | bytes 262144
  139.0 1.3 copy.24
  140.3 1.3 copy.25
